TPU v7x, 32 devices: a whole 2x2x4 slice. The times are simulated.
32 devices in a mesh: sp: 8 (over z, x), tp: 4 (over y, core).
Axes of the slice: x: 2, y: 2, z: 4, core: 2. Of those that a mesh axis runs over, the one named last changes fastest.
Arguments:
- queries: bfloat16 [1024, 32, 128], P('sp', 'tp'), may hold values from -6 to 6
- keys: bfloat16 [1024, 8, 128], P('sp', 'tp'), may hold values from -6 to 6
- values: bfloat16 [1024, 8, 128], P('sp', 'tp'), may hold values from -6 to 6
- q_gain: float32 [128], replicated, may hold values from 0.2 to 8
- k_gain: float32 [128], replicated, may hold values from 0.2 to 8
- w_out: bfloat16 [4096, 2048], P('tp'), may hold values from -0.09375 to 0.09375
- residual: bfloat16 [1024, 2048], P(('sp', 'tp')), may hold values from -6 to 6
- gain_mix: float32 [2048], replicated, may hold values from 0.1 to 1.9
- gain_pre: float32 [2048], replicated, may hold values from 0.1 to 1.9
- routes: int32 [1024, 4], P(('sp', 'tp')), may hold values from 0 to 7, all different within a row; in each aligned block of 32 rows (0 to 31, 32 to 63, ...) at most 32 rows name the same one
- route_weights: float32 [1024, 4], P(('sp', 'tp')), may hold values from 0.1 to 1
- w_gate: bfloat16 [8, 2048, 2048], P('sp', None, 'tp'), may hold values from -0.5 to 0.5
- w_up: bfloat16 [8, 2048, 2048], P('sp', None, 'tp'), may hold values from -0.5 to 0.5
- w_down: bfloat16 [8, 2048, 2048], P('sp', 'tp'), may hold values from -0.125 to 0.125
- gain_moe: float32 [2048], replicated, may hold values from 0.1 to 1.9
Outputs:
- layer_out: bfloat16 [1024, 2048], P(('sp', 'tp'))
Inputs may be any that keep to these rules, and one draw needn't show every extreme that they name: `routes`: each row names 4 different experts. In each aligned block of 32 rows (the rows of one device) no expert is named by more than 32 rows, a bound that some block reaches.
All inputs are finite; a program needn't handle non-finite values.
Results may differ from a plain program's by a relative error of at most 0.017.
The roundings to bfloat16 on the way count: a program that leaves them out, or rounds other values in their place, can miss the bound.
Values may be sent and summed in bfloat16 or wider, within the bound.
A program may use at most 128 MiB of HBM per device.

v0:
```python
import math

import jax
import jax.numpy as jnp
from jax import lax
from jax.sharding import PartitionSpec as P

TOP = 4
GRID_W = 64


norm_eps = 1e-06
rope_theta = 10000.0
clamp_limit = 7.0
swish_alpha = 1.702


def rope_tables(positions, head_size):
    row_index = (positions // GRID_W).astype(jnp.float32)
    col_index = (positions % GRID_W).astype(jnp.float32)
    freq_count = head_size // 4
    inverse = rope_theta ** (-jnp.arange(freq_count, dtype=jnp.float32) / freq_count)
    angles = jnp.stack([row_index[:, None] * inverse, col_index[:, None] * inverse], axis=1)
    return (jnp.cos(angles), jnp.sin(angles))


def turn(array_in, cosine_table, sine_table):
    token_count, head_count, head_size = array_in.shape
    split_field = array_in.reshape(token_count, head_count, 2, 2, head_size // 4)
    first_half = split_field[:, :, :, 0, :]
    second_half = split_field[:, :, :, 1, :]
    cos_wide = cosine_table[:, None]
    sin_wide = sine_table[:, None]
    turned = jnp.stack(
        [
            first_half * cos_wide - second_half * sin_wide,
            second_half * cos_wide + first_half * sin_wide,
        ],
        axis=3,
    )
    return turned.reshape(token_count, head_count, head_size)


def scale_rows(array_in, gain_vec):
    return (
        array_in
        * lax.rsqrt(jnp.mean(array_in * array_in, axis=-1, keepdims=True) + norm_eps)
        * gain_vec
    )


def slot_table(route_rows, experts, capacity):
    flat_routes = route_rows.reshape(-1)
    expert_hits = (flat_routes[:, None] == jnp.arange(experts, dtype=jnp.int32)[None, :]).astype(
        jnp.int32
    )
    slot_index = jnp.sum((jnp.cumsum(expert_hits, axis=0) - expert_hits) * expert_hits, axis=1)
    target = flat_routes * capacity + slot_index
    slot_onehot = target[:, None] == jnp.arange(experts * capacity, dtype=jnp.int32)[None, :]
    return slot_onehot.astype(jnp.bfloat16).reshape(
        route_rows.shape[0], route_rows.shape[1], experts * capacity
    )


def expert_apply(arrived_rows, w_gate, w_up, w_down):
    gate_pre = jnp.minimum(
        jnp.einsum("serd,edf->serf", arrived_rows, w_gate, preferred_element_type=jnp.float32),
        clamp_limit,
    )
    up_pre = jnp.clip(
        jnp.einsum("serd,edf->serf", arrived_rows, w_up, preferred_element_type=jnp.float32),
        -clamp_limit,
        clamp_limit,
    )
    active = (gate_pre * jax.nn.sigmoid(swish_alpha * gate_pre) * (up_pre + 1.0)).astype(
        jnp.bfloat16
    )
    partial_value = jnp.einsum("serf,efd->serd", active, w_down, preferred_element_type=jnp.float32)
    return lax.optimization_barrier(partial_value.astype(jnp.bfloat16)).astype(jnp.float32)


def send_back(finished):
    return lax.all_to_all(finished, "sp", split_axis=0, concat_axis=0, tiled=True)


def on_device(
    queries,
    keys,
    values,
    q_gain,
    k_gain,
    w_out,
    residual,
    gain_mix,
    gain_pre,
    routes,
    route_weights,
    w_gate,
    w_up,
    w_down,
    gain_moe,
):
    tok_rows, head_local, head_size = queries.shape
    kv_local = keys.shape[1]
    group_size = head_local // kv_local
    positions = lax.axis_index("sp") * tok_rows + jnp.arange(tok_rows, dtype=jnp.int32)
    cosine_table, sine_table = rope_tables(positions, head_size)
    q_turned = (
        turn(scale_rows(queries.astype(jnp.float32), q_gain), cosine_table, sine_table)
        * head_size ** (-0.5)
    ).astype(jnp.bfloat16)
    k_turned = turn(scale_rows(keys.astype(jnp.float32), k_gain), cosine_table, sine_table).astype(
        jnp.bfloat16
    )
    q_grouped = q_turned.reshape(tok_rows, kv_local, group_size, head_size)
    initial = (
        jnp.full((kv_local, group_size, tok_rows), -jnp.inf, jnp.float32),
        jnp.zeros((kv_local, group_size, tok_rows), jnp.float32),
        jnp.zeros((kv_local, group_size, tok_rows, head_size), jnp.float32),
    )
    carry_state = initial
    key_piece = lax.all_gather(k_turned, "sp", axis=0, tiled=True)
    value_piece = lax.all_gather(values, "sp", axis=0, tiled=True)
    piece_rows = key_piece.shape[0]
    block_rows = math.gcd(piece_rows, 1024)
    key_blocks = key_piece.reshape(piece_rows // block_rows, block_rows, kv_local, head_size)
    value_blocks = value_piece.reshape(piece_rows // block_rows, block_rows, kv_local, head_size)

    def absorb_block(state_now, key_value):
        running_max, running_sum, weighted = state_now
        key_block, value_block = key_value
        scores = jnp.einsum(
            "qkgd,skd->kgqs", q_grouped, key_block, preferred_element_type=jnp.float32
        )
        new_max = jnp.maximum(running_max, jnp.max(scores, axis=-1))
        rescale = jnp.exp(running_max - new_max)
        unnorm = jnp.exp(scores - new_max[..., None])
        running_sum = running_sum * rescale + jnp.sum(unnorm, axis=-1)
        weighted = weighted * rescale[..., None] + jnp.einsum(
            "kgqs,skd->kgqd",
            unnorm.astype(jnp.bfloat16),
            value_block,
            preferred_element_type=jnp.float32,
        )
        return ((new_max, running_sum, weighted), None)

    carry_state, ignored = lax.scan(absorb_block, carry_state, (key_blocks, value_blocks))
    running_max, running_sum, weighted = carry_state
    mixed_heads = (weighted / running_sum[..., None]).transpose(2, 0, 1, 3)
    mixed_heads = mixed_heads.reshape(tok_rows, head_local * head_size).astype(jnp.bfloat16)
    tok_part = residual.shape[0]
    width = residual.shape[1]
    projected = lax.psum_scatter(
        jnp.dot(mixed_heads, w_out, preferred_element_type=jnp.float32).astype(jnp.bfloat16),
        "tp",
        scatter_dimension=0,
        tiled=True,
    ).astype(jnp.float32)
    middle = residual.astype(jnp.float32) + scale_rows(projected, gain_mix)
    normed = scale_rows(middle, gain_pre).astype(jnp.bfloat16)
    local_experts = w_gate.shape[0]
    experts_all = local_experts * lax.axis_size("sp")
    capacity = max(2, (2 * tok_part * TOP + experts_all - 1) // experts_all)
    tables = slot_table(routes, experts_all, capacity)
    chosen = jnp.sum(tables, axis=1)
    outbound = jnp.einsum("tp,td->pd", chosen, normed, preferred_element_type=jnp.float32)
    outbound = outbound.astype(jnp.bfloat16).reshape(experts_all, capacity, width)
    arrived_rows = lax.all_gather(
        lax.all_to_all(outbound, "sp", split_axis=0, concat_axis=0, tiled=True),
        "tp",
        axis=0,
        tiled=True,
    )
    leading = arrived_rows.shape[0] // local_experts
    partial_value = expert_apply(
        arrived_rows.reshape(leading, local_experts, arrived_rows.shape[1], width),
        w_gate,
        w_up,
        w_down,
    )
    summed = lax.psum_scatter(
        partial_value.reshape(arrived_rows.shape).astype(jnp.bfloat16),
        "tp",
        scatter_dimension=0,
        tiled=True,
    )
    returned = send_back(summed)
    gathered = jnp.einsum(
        "tkp,pd->tkd",
        tables,
        returned.reshape(experts_all * capacity, width),
        preferred_element_type=jnp.float32,
    )
    mixture = jnp.sum(gathered * route_weights[:, :, None], axis=1)
    return (middle + scale_rows(mixture, gain_moe)).astype(jnp.bfloat16)


def solution(mesh):
    placed = (
        P("sp", "tp", None),
        P("sp", "tp", None),
        P("sp", "tp", None),
        P(),
        P(),
        P("tp", None),
        P(("sp", "tp"), None),
        P(),
        P(),
        P(("sp", "tp"), None),
        P(("sp", "tp"), None),
        P("sp", None, "tp"),
        P("sp", None, "tp"),
        P("sp", "tp", None),
        P(),
    )
    return jax.shard_map(
        on_device, mesh=mesh, in_specs=placed, out_specs=P(("sp", "tp"), None), check_vma=False
    )
```

profile of v0, /device:TPU:0, one launch (start us, length us, event | category | flops | bytes accessed | tf_op | source)
XLA Modules:
  0.0 267.1 jit_solution(2984971475194426291)
XLA Ops:
  6.5 0.0 reduce-scatter.3.cloned.1.call-start
  6.6 1.1 copy.57
  7.7 0.1 broadcast_multiply_fusion.1
  7.8 0.1 fusion.58
  7.9 0.7 fusion.46
  8.7 0.1 copy.58
  8.9 1.0 copy.61
  9.8 1.2 copy.59
  11.0 0.1 fusion.36
  11.1 0.8 fusion.37
  11.8 0.1 multiply_subtract_fusion
  11.9 29.6 %all_gather.10 = bf16[1024,2,128]{0,2,1:T(8,128)(2,1)S(1)} all-gather(bf16[128,2,128]{0,2,1:T(8,128)(2,1)S(1)} %copy.61), channel_id=1, replica_groups=mesh['sp'=8,'tp'=4] {'sp'}, dimensions={0}, use_global_device_ids=true | all-gather | bytes 589824 | tf_op jit(solution)/shard_map/all_gather | solution.py:123
  41.5 31.4 %all_gather.9 = bf16[1024,2,128]{2,0,1:T(8,128)(2,1)S(1)} all-gather(bf16[128,2,128]{2,0,1:T(8,128)(2,1)S(1)} %copy.58), channel_id=1, replica_groups=mesh['sp'=8,'tp'=4] {'sp'}, dimensions={0}, use_global_device_ids=true | all-gather | bytes 589824 | tf_op jit(solution)/shard_map/all_gather | solution.py:122
  72.9 0.1 fusion.38
  73.0 0.7 bitcast_reduce_fusion
  73.7 0.6 fusion.1
  74.3 0.0 copy-start.1
  74.3 0.9 fusion.31
  75.2 1.3 copy-done.1
  76.5 1.5 convolution_convert_fusion.1
  78.1 0.0 reduce-scatter.3.cloned.1.call-update
  78.1 0.0 all-gather.2.cloned.1.call-start
  78.2 0.1 copy.63
  78.2 0.1 eq.53
  78.4 0.1 fusion.56
  78.5 0.2 reduce_window_sum.11
  78.6 0.2 select_reduce_fusion
  78.8 0.1 reduce_sum.95
  78.9 0.1 copy.64
  79.0 0.1 fusion.54
  79.1 20.0 %reduce-scatter.3.cloned.1.call-done = bf16[32,2048]{1,0:T(8,128)(2,1)} async-done(((bf16[128,2048]{1,0:T(8,128)(2,1)}), bf16[32,2048]{1,0:T(8,128)(2,1)}) %reduce-scatter.3.cloned.1.call-update) | async-done | bytes 131088 | tf_op jit(solution)/shard_map/reduce_scatter | solution.py:153
  99.1 1.0 fusion.42
  100.2 1.1 multiply_reduce_fusion.1
  101.4 1.4 convolution_convert_fusion
  102.8 31.0 %all_to_all.10 = bf16[8,32,2048]{2,1,0:T(8,128)(2,1)} all-to-all(bf16[8,32,2048]{2,1,0:T(8,128)(2,1)S(1)} %bitcast.129), channel_id=1, replica_groups=mesh['sp'=8,'tp'=4] {'sp'}, dimensions={0} | all-to-all | bytes 2097152 | tf_op jit(solution)/shard_map/all_to_all | solution.py:169
  133.8 0.0 all-gather.2.cloned.1.call-update
  133.8 0.0 reduce-scatter.5.cloned.1.call-start
  133.8 32.6 %all-gather.2.cloned.1.call-done = bf16[32,32,2048]{2,1,0:T(8,128)(2,1)} async-done(((bf16[8,32,2048]{2,1,0:T(8,128)(2,1)}), bf16[32,32,2048]{2,1,0:T(8,128)(2,1)}) %all-gather.2.cloned.1.call-update) | async-done | bytes 4194320 | tf_op jit(solution)/shard_map/all_gather | solution.py:168
  166.5 6.6 %fusion.7 = f32[32,32,512]{2,1,0:T(8,128)} fusion(bf16[32,32,2048]{2,1,0:T(8,128)(2,1)} %all-gather.2.cloned.1.call-done, bf16[1,2048,512]{2,1,0:T(8,128)(2,1)} %param.27), kind=kOutput, calls=%fused_computation.13 | convolution fusion | flops 2147483648 | bytes 8388608 | tf_op jit(solution)/shard_map/serd,edf->serf/dot_general | solution.py:71
  173.1 10.3 %convert_bitcast_fusion = bf16[32,1,32,2048]{3,2,0,1:T(8,128)(2,1)} fusion(bf16[1,512,2048]{2,1,0:T(8,128)(2,1)S(1)} %copy-done, f32[32,32,512]{2,1,0:T(8,128)} %fusion.7, bf16[32,32,2048]{2,1,0:T(8,128)(2,1)} %all-gather.2.cloned.1.call-done, bf16[1,2048,512]{2,1,0:T(8,128)(2,1)} %param.26), kind=kOutput, calls=%fused_computation.3 | convolution fusion | flops 4302307328 | bytes 14680064 | tf_op jit(solution)/shard_map/serf,efd->serd/dot_general | solution.py:78
  183.4 0.0 reduce-scatter.5.cloned.1.call-update
  183.4 0.0 copy-start.8
  183.4 0.0 copy-start.6
  183.4 44.7 %reduce-scatter.5.cloned.1.call-done = bf16[8,32,2048]{2,1,0:T(8,128)(2,1)} async-done(((bf16[32,32,2048]{2,1,0:T(8,128)(2,1)}), bf16[8,32,2048]{2,1,0:T(8,128)(2,1)}) %reduce-scatter.5.cloned.1.call-update) | async-done | bytes 1048592 | tf_op jit(solution)/shard_map/reduce_scatter | solution.py:181
  228.1 31.1 %all_to_all.11 = bf16[8,32,2048]{2,1,0:T(8,128)(2,1)S(1)} all-to-all(bf16[8,32,2048]{2,1,0:T(8,128)(2,1)} %reduce-scatter.5.cloned.1.call-done), channel_id=1, replica_groups=mesh['sp'=8,'tp'=4] {'sp'}, dimensions={0} | all-to-all | bytes 2097152 | tf_op jit(solution)/shard_map/all_to_all | solution.py:83
  259.2 0.3 fusion.21
  259.6 0.1 multiply_reduce_fusion
  259.8 0.8 add_convert_fusion
  (27 shorter events, 0.2 us)
Async XLA Ops:
  6.5 166.5 %copy-start = (bf16[1,512,2048]{2,1,0:T(8,128)(2,1)S(1)}, bf16[1,512,2048]{2,1,0:T(8,128)(2,1)}, u32[]{:S(2)}) copy-start(bf16[1,512,2048]{2,1,0:T(8,128)(2,1)} %param.28) | copy-start | bytes 6291460
  6.5 92.6 %reduce-scatter.3.cloned.1.call-start = ((), (), s32[]{:S(2)}) async-start(), calls=%async_computation.4 | async-start | bytes 655360 | tf_op jit(solution)/shard_map/reduce_scatter | solution.py:153
  74.3 2.2 copy-start.1
  76.5 1.6 copy-start.7
  76.5 23.6 %copy-start.3 = (bf16[32,2048]{1,0:T(8,128)(2,1)S(1)}, bf16[32,2048]{1,0:T(8,128)(2,1)}, u32[]{:S(2)}) copy-start(bf16[32,2048]{1,0:T(8,128)(2,1)} %param.21) | copy-start | bytes 393220
  76.5 23.7 %copy-start.4 = (f32[2048]{0:T(1024)S(1)}, f32[2048]{0:T(1024)}, u32[]{:S(2)}) copy-start(f32[2048]{0:T(1024)} %param.22) | copy-start | bytes 24580
  76.5 24.8 %copy-start.5 = (f32[2048]{0:T(1024)S(1)}, f32[2048]{0:T(1024)}, u32[]{:S(2)}) copy-start(f32[2048]{0:T(1024)} %param.23) | copy-start | bytes 24580
  78.1 88.4 %all-gather.2.cloned.1.call-start = ((), (), s32[]{:S(2)}) async-start(), calls=%async_computation.5 | async-start | bytes 5242880 | tf_op jit(solution)/shard_map/all_gather | solution.py:168
  133.8 94.3 %reduce-scatter.5.cloned.1.call-start = ((), (), s32[]{:S(2)}) async-start(), calls=%async_computation.6 | async-start | bytes 5242880 | tf_op jit(solution)/shard_map/reduce_scatter | solution.py:181
  183.4 75.8 %copy-start.8 = (f32[32,4]{0,1:T(4,128)S(1)}, f32[32,4]{0,1:T(4,128)}, u32[]{:S(2)}) copy-start(f32[32,4]{0,1:T(4,128)} %param.25) | copy-start | bytes 1540
  183.4 76.3 %copy-start.2 = (bf16[32,2048]{1,0:T(8,128)(2,1)S(1)}, bf16[32,2048]{1,0:T(8,128)(2,1)}, u32[]{:S(2)}) copy-start(bf16[32,2048]{1,0:T(8,128)(2,1)} %reduce-scatter.3.cloned.1.call-done) | copy-start | bytes 393220
  183.4 76.3 %copy-start.6 = (f32[2048]{0:T(1024)S(1)}, f32[2048]{0:T(1024)}, u32[]{:S(2)}) copy-start(f32[2048]{0:T(1024)} %param.29) | copy-start | bytes 24580
Sparse Core Ops, SparseCore 0:
  78.2 20.8 reduce-scatter.2
  133.9 32.5 all-gather.1
  183.5 44.5 reduce-scatter.4
where the time goes:
time: 268 us; the launch traced here: 267 us
  blocking collectives  123 us (46%)
  waiting for transfers between devices  97.4 us (36%)
  matrix products  21.8 us (8%)
  between operations  13.4 us (5%)
  other arithmetic  6.28 us (2%)
  local copies, waits for them, and re-layouts  5.04 us (2%)
    reduce_scatter x1, waiting for transfers between devices, on_device(): lax.psum_scatter(partial_value.reshape(arrived_rows.shape).astype(jnp.bfl...  44.7 us
    all_gather x1, waiting for transfers between devices, on_device(): lax.all_gather(lax.all_to_all(outbound, 'sp', split_axis=0, concat_axis=0...  32.6 us
    all_gather x1, blocking collectives, on_device(): key_piece = lax.all_gather(k_turned, 'sp', axis=0, tiled=True)  31.4 us
    all_to_all x1, blocking collectives, send_back(): lax.all_to_all(finished, 'sp', split_axis=0, concat_axis=0, tiled=True)  31.1 us
    all_to_all x1, blocking collectives, on_device(): lax.all_to_all(outbound, 'sp', split_axis=0, concat_axis=0, tiled=True)  31 us
    all_gather x1, blocking collectives, on_device(): value_piece = lax.all_gather(values, 'sp', axis=0, tiled=True)  29.6 us
    reduce_scatter x1, waiting for transfers between devices, on_device(): lax.psum_scatter(jnp.dot(mixed_heads, w_out, preferred_element_type=jnp.f...  20 us
    dot_general x1, matrix products, expert_apply(): jnp.einsum('serf,efd->serd', active, w_down, preferred_element_type=jnp.f...  10.3 us
  transfers between devices with their start and end apart: 3, of which 3 were waited for; matrix products, arithmetic and copies ran while one was open for 0% of the time, Pallas kernels for 0%

commit v1 on v0

--- a/solution.py
+++ b/solution.py
@@ -1,8 +1,11 @@
+import functools
 import math
 
 import jax
 import jax.numpy as jnp
 from jax import lax
+from jax.experimental import pallas as pl
+from jax.experimental.pallas import tpu as pltpu
 from jax.sharding import PartitionSpec as P
 
 TOP = 4
@@ -81,6 +84,333 @@
 
 def send_back(finished):
     return lax.all_to_all(finished, "sp", split_axis=0, concat_axis=0, tiled=True)
+
+
+MESH = pl.DeviceIdType.MESH
+RING = 4
+PAIR = 2
+LANES = 128
+
+
+def gather_kernel(n, own_ref, out_ref, send_sem, recv_sem, own_sem):
+    me = lax.axis_index("sp")
+    tp = lax.axis_index("tp")
+    barrier = pltpu.get_barrier_semaphore()
+
+    def greet(i, carry):
+        pl.semaphore_signal(
+            barrier, inc=1, device_id=(lax.rem(me + i, n), tp), device_id_type=MESH
+        )
+        return carry
+
+    lax.fori_loop(1, n, greet, 0)
+    keep = pltpu.make_async_copy(own_ref, out_ref.at[me], own_sem)
+    keep.start()
+    pl.semaphore_wait(barrier, n - 1)
+
+    def copy_of(i):
+        return pltpu.make_async_remote_copy(
+            src_ref=own_ref,
+            dst_ref=out_ref.at[me],
+            send_sem=send_sem.at[i],
+            recv_sem=recv_sem.at[i],
+            device_id=(lax.rem(me + i, n), tp),
+            device_id_type=MESH,
+        )
+
+    def start(i, carry):
+        copy_of(i).start()
+        return carry
+
+    def finish(i, carry):
+        copy_of(i).wait()
+        return carry
+
+    lax.fori_loop(1, n, start, 0)
+    keep.wait()
+    lax.fori_loop(1, n, finish, 0)
+
+
+def gather_sp(block):
+    n = lax.axis_size("sp")
+    return pl.pallas_call(
+        functools.partial(gather_kernel, n),
+        out_shape=jax.ShapeDtypeStruct((n,) + block.shape, block.dtype),
+        in_specs=[pl.BlockSpec(memory_space=pltpu.VMEM)],
+        out_specs=pl.BlockSpec(memory_space=pltpu.VMEM),
+        scratch_shapes=[
+            pltpu.SemaphoreType.DMA((n,)),
+            pltpu.SemaphoreType.DMA((n,)),
+            pltpu.SemaphoreType.DMA,
+        ],
+        compiler_params=pltpu.CompilerParams(collective_id=0, has_side_effects=True),
+        cost_estimate=pl.CostEstimate(flops=0, bytes_accessed=1 << 24, transcendentals=0),
+        name="gather_kv",
+    )(block)
+
+
+def wide(value):
+    return value.astype(jnp.float32)
+
+
+def experts_kernel(
+    part, residual, gain_mix, gain_pre, gain_moe, tail, wg_hbm, wu_hbm, wd_hbm, out,
+    wg, wu, wd, got, middle, rows, active, partial, core_in, summed, far_in, near_in,
+    x_in, y_in, w_sem, part_s, part_r, y_s, y_r, x_s, x_r, z_s, z_r, q_s, q_r, c_s, c_r,
+    rc_s, rc_r, e_s, e_r, f_s, f_r, l_s, l_r, rx_s, rx_r, ry_s, ry_r,
+):
+    sp = lax.axis_index("sp")
+    tp = lax.axis_index("tp")
+    z, x = sp // PAIR, lax.rem(sp, PAIR)
+    y, c = tp // PAIR, lax.rem(tp, PAIR)
+    ox, oy, oc = 1 - x, 1 - y, 1 - c
+    zp, zm, zq = lax.rem(z + 1, RING), lax.rem(z + 3, RING), lax.rem(z + 2, RING)
+    width = residual.shape[1]
+    to_c = (sp, y * PAIR + oc)
+    to_y = (sp, oy * PAIR + c)
+    to_yc = (sp, oy * PAIR + oc)
+    to_x = (z * PAIR + ox, tp)
+    to_zp = (zp * PAIR + x, tp)
+    to_zm = (zm * PAIR + x, tp)
+    peers = (to_c, to_y, to_yc, to_x, to_zp, to_zm)
+
+    loads = [
+        pltpu.make_async_copy(a, b, w_sem.at[i])
+        for i, (a, b) in enumerate(((wg_hbm, wg), (wu_hbm, wu), (wd_hbm, wd)))
+    ]
+    for load in loads:
+        load.start()
+    barrier = pltpu.get_barrier_semaphore()
+    for peer in peers:
+        pl.semaphore_signal(barrier, inc=1, device_id=peer, device_id_type=MESH)
+    pl.semaphore_wait(barrier, len(peers))
+
+    started = []
+
+    def send(src, dst, s, r, to):
+        copy = pltpu.make_async_remote_copy(
+            src_ref=src, dst_ref=dst, send_sem=s, recv_sem=r, device_id=to, device_id_type=MESH
+        )
+        copy.start()
+        started.append(copy)
+        return copy
+
+    with jax.named_scope("proj"):
+        copies = [
+            send(part.at[to[1]], core_in.at[0, i], part_s.at[i], part_r.at[i], to)
+            for i, to in ((2, to_yc), (1, to_y), (0, to_c))
+        ]
+        for copy in copies:
+            copy.wait_recv()
+        projected = wide(part[tp])
+        for i in range(3):
+            projected = projected + wide(core_in[0, i])
+        mid = wide(residual[...]) + scale_rows(projected, gain_mix[...])
+        middle[...] = mid
+        mine = x * PAIR + y
+        got[z, c, mine, :, 0:width] = scale_rows(mid, gain_pre[...]).astype(jnp.bfloat16)
+        got[z, c, mine, :, width:] = tail[...]
+
+    blk = (mine, x * PAIR + oy, ox * PAIR + y, ox * PAIR + oy)
+    groups = (z, zm, zp, zq)
+
+    def block(g, k):
+        return got.at[groups[g], c, blk[k]]
+
+    def relay(g, k):
+        return send(block(g, k), block(g, k), c_s.at[g, k], c_r.at[g, k], to_c)
+
+    relays = [[None] * 4 for _ in range(4)]
+    plus, minus = [None] * 4, [None] * 4
+    far = [None] * 4
+
+    def spread(k):
+        plus[k] = send(block(0, k), block(0, k), z_s.at[0, k], z_r.at[0, k], to_zp)
+        minus[k] = send(block(0, k), block(0, k), z_s.at[1, k], z_r.at[1, k], to_zm)
+        relays[0][k] = relay(0, k)
+
+    with jax.named_scope("spread"):
+        ycopy = send(block(0, 0), block(0, 0), y_s.at[0], y_r.at[0], to_y)
+        xcopy0 = send(block(0, 0), block(0, 0), x_s.at[0], x_r.at[0], to_x)
+        spread(0)
+        ycopy.wait_recv()
+        xcopy1 = send(block(0, 1), block(0, 1), x_s.at[1], x_r.at[1], to_x)
+        spread(1)
+        xcopy0.wait_recv()
+        spread(2)
+        xcopy1.wait_recv()
+        spread(3)
+
+    per = got.shape[2] * got.shape[3]
+
+    def serve(g):
+        group = groups[g]
+        arrived = got[group].reshape(2 * per, got.shape[4])
+        rows[...] = arrived
+        spread_w = wide(rows[:, width:])
+        lane = lax.broadcasted_iota(jnp.int32, spread_w.shape, 1)
+        chosen = lax.rem(lane, spread_w.shape[1] // 2) == sp
+        coef = jnp.sum(jnp.where(chosen, spread_w, 0.0), axis=1, keepdims=True)
+        step = min(wg.shape[1], 256)
+
+        @pl.loop(0, wg.shape[1] // step)
+        def _(i):
+            cols = pl.ds(pl.multiple_of(i * step, step), step)
+            gate = jnp.dot(rows[:, 0:width], wg[:, cols], preferred_element_type=jnp.float32)
+            up = jnp.dot(rows[:, 0:width], wu[:, cols], preferred_element_type=jnp.float32)
+            gate = jnp.minimum(gate, clamp_limit)
+            up = jnp.clip(up, -clamp_limit, clamp_limit)
+            active[:, cols] = (gate * jax.nn.sigmoid(swish_alpha * gate) * (up + 1.0)).astype(
+                jnp.bfloat16
+            )
+
+        @pl.loop(0, width // 512)
+        def _(i):
+            cols = pl.ds(pl.multiple_of(i * 512, 512), 512)
+            down = jnp.dot(active[...], wd[:, cols], preferred_element_type=jnp.float32)
+            partial[g, :, :, :, cols] = (
+                (down * coef).astype(jnp.bfloat16).reshape(partial.shape[1:4] + (512,))
+            )
+
+        return send(partial.at[g, oc], core_in.at[g], rc_s.at[g], rc_r.at[g], to_c)
+
+    def fold(g, copy):
+        copy.wait_recv()
+        for k in range(4):
+            summed[g, k] = (wide(partial[g, c, k]) + wide(core_in[g, k])).astype(jnp.bfloat16)
+
+    def await_core(g):
+        for k in range(4):
+            relays[g][k].wait_recv()
+
+    half_a, half_b = pl.ds(x * PAIR, PAIR), pl.ds(ox * PAIR, PAIR)
+
+    for load in loads:
+        load.wait()
+    with jax.named_scope("own"):
+        await_core(0)
+        back0 = serve(0)
+    with jax.named_scope("near"):
+        for k in range(4):
+            plus[k].wait_recv()
+            if k < 2:
+                far[k] = send(block(1, k), block(1, k), q_s.at[k], q_r.at[k], to_zp)
+            relays[1][k] = relay(1, k)
+            minus[k].wait_recv()
+            if k >= 2:
+                far[k] = send(block(2, k), block(2, k), q_s.at[k], q_r.at[k], to_zm)
+            relays[2][k] = relay(2, k)
+        await_core(1)
+        back1 = serve(1)
+        fold(0, back0)
+        for k in range(4):
+            far[k].wait_recv()
+            relays[3][k] = relay(3, k)
+        await_core(2)
+        back2 = serve(2)
+        fold(1, back1)
+        early_m = send(
+            summed.at[1, half_a], near_in.at[1, half_a], e_s.at[1], e_r.at[1], to_zm
+        )
+    with jax.named_scope("far"):
+        await_core(3)
+        back3 = serve(3)
+        fold(2, back2)
+        early_p = send(
+            summed.at[2, half_b], near_in.at[0, half_b], e_s.at[0], e_r.at[0], to_zp
+        )
+        fold(3, back3)
+        far_p = send(summed.at[3, half_a], far_in.at[0], f_s.at[0], f_r.at[0], to_zp)
+        far_m = send(summed.at[3, half_b], far_in.at[1], f_s.at[1], f_r.at[1], to_zm)
+    with jax.named_scope("back"):
+        far_p.wait_recv()
+        for k in range(2):
+            place = x * PAIR + k
+            summed[2, place] = (wide(summed[2, place]) + wide(far_in[0, k])).astype(jnp.bfloat16)
+        late_p = send(
+            summed.at[2, half_a], near_in.at[0, half_a], l_s.at[0], l_r.at[0], to_zp
+        )
+        far_m.wait_recv()
+        for k in range(2):
+            place = ox * PAIR + k
+            summed[1, place] = (wide(summed[1, place]) + wide(far_in[1, k])).astype(jnp.bfloat16)
+        late_m = send(
+            summed.at[1, half_b], near_in.at[1, half_b], l_s.at[1], l_r.at[1], to_zm
+        )
+
+        def total(place):
+            return wide(summed[0, place]) + wide(near_in[0, place]) + wide(near_in[1, place])
+
+        early_p.wait_recv()
+        early_m.wait_recv()
+        late_m.wait_recv()
+        late_p.wait_recv()
+        for k in range(2):
+            place = ox * PAIR + k
+            summed[0, place] = total(place).astype(jnp.bfloat16)
+        xback = send(summed.at[0, half_b], x_in, rx_s.at[0], rx_r.at[0], to_x)
+        xback.wait_recv()
+        summed[0, blk[1]] = (total(blk[1]) + wide(x_in[oy])).astype(jnp.bfloat16)
+        yback = send(summed.at[0, blk[1]], y_in, ry_s.at[0], ry_r.at[0], to_y)
+        keep = total(mine) + wide(x_in[y])
+        yback.wait_recv()
+        mixture = keep + wide(y_in[...])
+        out[...] = (middle[...] + scale_rows(mixture, gain_moe[...])).astype(out.dtype)
+        for copy in started:
+            copy.wait_send()
+
+
+def experts_layer(part, residual, gain_mix, gain_pre, gain_moe, tail, w_gate, w_up, w_down):
+    tok, width = residual.shape
+    ff = w_gate.shape[1]
+    full = width + tail.shape[1]
+    blocks = PAIR * PAIR
+    bf, f32 = jnp.bfloat16, jnp.float32
+    dma = pltpu.SemaphoreType.DMA
+    here = pl.BlockSpec(memory_space=pltpu.VMEM)
+    there = pl.BlockSpec(memory_space=pl.ANY)
+    sems = []
+    for dims in (
+        (3,), (1,), (2,), (2, 4), (4,), (4, 4), (4,), (2,), (2,), (2,), (1,), (1,)
+    ):
+        sems += [dma(dims), dma(dims)]
+    return pl.pallas_call(
+        experts_kernel,
+        out_shape=jax.ShapeDtypeStruct((tok, width), bf),
+        in_specs=[here] * 6 + [there] * 3,
+        out_specs=here,
+        scratch_shapes=[
+            pltpu.VMEM((width, ff), bf),
+            pltpu.VMEM((width, ff), bf),
+            pltpu.VMEM((ff, width), bf),
+            pltpu.VMEM((RING, PAIR, blocks, tok, full), bf),
+            pltpu.VMEM((tok, width), f32),
+            pltpu.VMEM((PAIR * blocks * tok, full), bf),
+            pltpu.VMEM((PAIR * blocks * tok, ff), bf),
+            pltpu.VMEM((RING, PAIR, blocks, tok, width), bf),
+            pltpu.VMEM((RING, blocks, tok, width), bf),
+            pltpu.VMEM((RING, blocks, tok, width), bf),
+            pltpu.VMEM((2, PAIR, tok, width), bf),
+            pltpu.VMEM((2, blocks, tok, width), bf),
+            pltpu.VMEM((PAIR, tok, width), bf),
+            pltpu.VMEM((tok, width), bf),
+            dma((3,)),
+        ]
+        + sems,
+        compiler_params=pltpu.CompilerParams(
+            collective_id=1, has_side_effects=True, vmem_limit_bytes=56 << 20
+        ),
+        name="experts_layer",
+    )(part, residual, gain_mix, gain_pre, gain_moe, tail, w_gate, w_up, w_down)
+
+
+def weight_tail(routes, route_weights, experts):
+    hits = routes[:, :, None] == jnp.arange(experts, dtype=jnp.int32)[None, None, :]
+    coef = jnp.sum(jnp.where(hits, route_weights[:, :, None], 0.0), axis=1)
+    high = lax.reduce_precision(coef, 8, 7)
+    low = coef - high
+    gap = jnp.zeros((coef.shape[0], LANES // 2 - experts), jnp.float32)
+    return jnp.concatenate([high, gap, low, gap], axis=1).astype(jnp.bfloat16)
 
 
 def on_device(
@@ -119,8 +449,14 @@
         jnp.zeros((kv_local, group_size, tok_rows, head_size), jnp.float32),
     )
     carry_state = initial
-    key_piece = lax.all_gather(k_turned, "sp", axis=0, tiled=True)
-    value_piece = lax.all_gather(values, "sp", axis=0, tiled=True)
+    kv_cols = kv_local * head_size
+    both = gather_sp(
+        jnp.concatenate(
+            [k_turned.reshape(tok_rows, kv_cols), values.reshape(tok_rows, kv_cols)], axis=1
+        )
+    ).reshape(-1, 2 * kv_cols)
+    key_piece = both[:, :kv_cols].reshape(-1, kv_local, head_size)
+    value_piece = both[:, kv_cols:].reshape(-1, kv_local, head_size)
     piece_rows = key_piece.shape[0]
     block_rows = math.gcd(piece_rows, 1024)
     key_blocks = key_piece.reshape(piece_rows // block_rows, block_rows, kv_local, head_size)
@@ -150,17 +486,31 @@
     mixed_heads = mixed_heads.reshape(tok_rows, head_local * head_size).astype(jnp.bfloat16)
     tok_part = residual.shape[0]
     width = residual.shape[1]
+    part = jnp.dot(mixed_heads, w_out, preferred_element_type=jnp.float32).astype(jnp.bfloat16)
+    local_experts = w_gate.shape[0]
+    experts_all = local_experts * lax.axis_size("sp")
+    capacity = max(2, (2 * tok_part * TOP + experts_all - 1) // experts_all)
+    grid_fits = lax.axis_size("sp") == RING * PAIR and lax.axis_size("tp") == PAIR * PAIR
+    if grid_fits and local_experts == 1 and capacity >= tok_part:
+        return experts_layer(
+            part.reshape(PAIR * PAIR, tok_part, width),
+            residual,
+            gain_mix[None],
+            gain_pre[None],
+            gain_moe[None],
+            weight_tail(routes, route_weights, experts_all),
+            w_gate[0],
+            w_up[0],
+            w_down[0],
+        )
     projected = lax.psum_scatter(
-        jnp.dot(mixed_heads, w_out, preferred_element_type=jnp.float32).astype(jnp.bfloat16),
+        part,
         "tp",
         scatter_dimension=0,
         tiled=True,
     ).astype(jnp.float32)
     middle = residual.astype(jnp.float32) + scale_rows(projected, gain_mix)
     normed = scale_rows(middle, gain_pre).astype(jnp.bfloat16)
-    local_experts = w_gate.shape[0]
-    experts_all = local_experts * lax.axis_size("sp")
-    capacity = max(2, (2 * tok_part * TOP + experts_all - 1) // experts_all)
     tables = slot_table(routes, experts_all, capacity)
     chosen = jnp.sum(tables, axis=1)
     outbound = jnp.einsum("tp,td->pd", chosen, normed, preferred_element_type=jnp.float32)

time: 268 us -> 144 us (0.54)
  Pallas kernels: 0 us -> 130 us
  blocking collectives: 123 us -> 0 us
  waiting for transfers between devices: 97.4 us -> 0 us
  matrix products: 21.8 us -> 3.21 us
  between operations: 13.4 us -> 0.23 us
  other arithmetic: 6.28 us -> 3.31 us
    pallas_call x0 -> x2, Pallas kernels: none -> 130 us  [the longest x1 106 us: experts_layer(): pl.pallas_call(experts_kernel, out_shape=jax.ShapeDtypeStruct((tok, width...]
    reduce_scatter x2 -> x0, waiting for transfers between devices: 64.7 us -> none  [the longest x1 44.7 us: on_device(): lax.psum_scatter(partial_value.reshape(arrived_rows.shape).astype(jnp.bfl...]
    all_to_all x2 -> x0, blocking collectives: 62.1 us -> none  [the longest x1 31.1 us: send_back(): lax.all_to_all(finished, 'sp', split_axis=0, concat_axis=0, tiled=True)]
    all_gather x2 -> x0, blocking collectives: 61 us -> none  [the longest x1 31.4 us: on_device(): key_piece = lax.all_gather(k_turned, 'sp', axis=0, tiled=True)]
    all_gather x1 -> x0, waiting for transfers between devices: 32.6 us -> none  [on_device(): lax.all_gather(lax.all_to_all(outbound, 'sp', split_axis=0, concat_axis=0...]
    dot_general x4 -> x0, matrix products: 18.6 us -> none  [the longest x1 10.3 us: expert_apply(): jnp.einsum('serf,efd->serd', active, w_down, preferred_element_type=jnp.f...]
  transfers between devices with their start and end apart: 3 -> 0, of which waited for: 3 -> 0; matrix products, arithmetic and copies ran while one was open for 0% -> 0% of each run, Pallas kernels for 0% -> 0%
where the time goes in v1:
time: 144 us; the launch traced here: 143 us
  Pallas kernels  130 us (90%)
  local copies, waits for them, and re-layouts  6.25 us (4%)
  other arithmetic  3.31 us (2%)
  matrix products  3.21 us (2%)
    pallas_call x1, Pallas kernels, experts_layer(): pl.pallas_call(experts_kernel, out_shape=jax.ShapeDtypeStruct((tok, width...  106 us
    pallas_call x1, Pallas kernels, gather_sp(): pl.pallas_call(functools.partial(gather_kernel, n), out_shape=jax.ShapeDt...  24.9 us
    unnamed x15, local copies, waits for them, and re-layouts  4.52 us

profile of v1, /device:TPU:0, one launch (start us, length us, event | category | flops | bytes accessed | tf_op | source)
XLA Modules:
  0.0 143.5 jit_solution(18201624517068343207)
XLA Ops:
  0.0 0.0 copy-start.1
  0.0 0.0 copy-start.4
  0.0 0.9 copy.62
  0.9 1.0 copy.42
  1.9 0.7 fusion.22
  2.7 0.1 broadcast_multiply_fusion.1
  2.8 0.1 fusion.24
  3.0 0.1 copy.43
  3.1 0.7 pad_maximum_fusion.own_ref
  3.7 24.9 %gather_kv.1 = bf16[8,128,512]{2,1,0:T(8,128)(2,1)} custom-call(bf16[128,512]{1,0:T(8,128)(2,1)} %pad_maximum_fusion.own_ref), custom_call_target="tpu_custom_call" | custom-call | bytes 16777216 | tf_op jit(solution)/shard_map/gather_kv/pallas_call | solution.py:136
  28.6 1.3 fusion.27
  29.9 0.2 copy.48
  30.1 0.2 copy.59
  30.3 0.0 copy-done.1
  30.3 0.2 copy.45
  30.6 0.1 fusion.18
  30.7 0.0 copy-done.4
  30.7 0.1 fusion.19
  30.8 0.1 multiply_subtract_fusion
  30.9 0.1 fusion.20
  30.9 0.8 bitcast_reduce_fusion
  31.7 0.0 copy-start
  31.7 0.6 fusion.1
  32.3 0.0 copy-start.2
  32.3 0.0 copy-start.3
  32.4 0.9 fusion.15
  33.3 0.6 copy-done
  33.9 1.5 %convolution_convert_fusion = bf16[128,2048]{1,0:T(8,128)(2,1)} fusion(bf16[128,1024]{0,1:T(8,128)(2,1)S(1)} %bitcast.74, bf16[1024,2048]{1,0:T(8,128)(2,1)S(1)} %copy-done), kind=kOutput, calls=%fused_computation.5 | convolution fusion | flops 537133056 | bytes 4980736 | tf_op jit(solution)/shard_map/dot_general | solution.py:489
  35.4 0.0 copy-done.2
  35.4 0.0 copy-done.3
  35.5 0.1 copy.50
  35.5 0.1 copy.51
  35.6 0.7 pad_maximum_fusion.3.tail
  36.3 105.6 %experts_layer.1 = bf16[32,2048]{1,0:T(8,128)(2,1)} custom-call(bf16[4,32,2048]{2,1,0:T(8,128)(2,1)} %bitcast.68, bf16[32,2048]{1,0:T(8,128)(2,1)} %residual.1, f32[1,2048]{1,0:T(1,128)} %bitcast.78, f32[1,2048]{1,0:T(1,128)} %bitcast.79, f32[1,2048]{1,0:T(1,128)} %bitcast.80, bf16[32,128]{1,0:T(8,128)(2,1)} %pad_maximum_fusion.3.tail, ...), custom_call_target="tpu_custom_call" | custom-call | tf_op jit(solution)/shard_map/experts_layer/pallas_call | solution.py:377
  141.9 1.6 %copy.64 = bf16[32,2048]{1,0:T(8,128)(2,1)} copy(bf16[32,2048]{1,0:T(8,128)(2,1)} %experts_layer.1) | data formatting | bytes 262144
  (13 shorter events, 0.1 us)
Async XLA Ops:
  0.0 30.3 %copy-start.1 = (bf16[128,8,128]{2,1,0:T(8,128)(2,1)S(1)}, bf16[128,8,128]{2,1,0:T(8,128)(2,1)}, u32[]{:S(2)}) copy-start(bf16[128,8,128]{2,1,0:T(8,128)(2,1)} %param.15) | copy-start | bytes 786436
  0.0 30.7 %copy-start.4 = (f32[128]{0:T(128)S(1)}, f32[128]{0:T(128)}, u32[]{:S(2)}) copy-start(f32[128]{0:T(128)} %param.18) | copy-start | bytes 1540
  31.7 2.2 %copy-start = (bf16[1024,2048]{1,0:T(8,128)(2,1)S(1)}, bf16[1024,2048]{1,0:T(8,128)(2,1)}, u32[]{:S(2)}) copy-start(bf16[1024,2048]{1,0:T(8,128)(2,1)} %param.20) | copy-start | bytes 12582916
  32.3 3.1 %copy-start.2 = (f32[32,4]{0,1:T(4,128)S(1)}, f32[32,4]{0,1:T(4,128)}, u32[]{:S(2)}) copy-start(f32[32,4]{0,1:T(4,128)} %param.25) | copy-start | bytes 1540
  32.3 3.1 %copy-start.3 = (s32[32,4]{0,1:T(4,128)S(1)}, s32[32,4]{0,1:T(4,128)}, u32[]{:S(2)}) copy-start(s32[32,4]{0,1:T(4,128)} %param.24) | copy-start | bytes 1540

commit v2 on v1

--- a/solution.py
+++ b/solution.py
@@ -92,43 +92,67 @@
 LANES = 128
 
 
-def gather_kernel(n, own_ref, out_ref, send_sem, recv_sem, own_sem):
+def gather_kernel(n, own_ref, out_ref, send_sem, recv_sem, pass_sem, take_sem, own_sem):
     me = lax.axis_index("sp")
     tp = lax.axis_index("tp")
+    pair = me + 1 - 2 * lax.rem(me, 2)
     barrier = pltpu.get_barrier_semaphore()
 
     def greet(i, carry):
         pl.semaphore_signal(
-            barrier, inc=1, device_id=(lax.rem(me + i, n), tp), device_id_type=MESH
+            barrier, inc=1, device_id=(lax.rem(me + 2 * i, n), tp), device_id_type=MESH
         )
         return carry
 
-    lax.fori_loop(1, n, greet, 0)
+    lax.fori_loop(1, n // 2, greet, 0)
+    pl.semaphore_signal(barrier, inc=1, device_id=(pair, tp), device_id_type=MESH)
     keep = pltpu.make_async_copy(own_ref, out_ref.at[me], own_sem)
     keep.start()
-    pl.semaphore_wait(barrier, n - 1)
-
-    def copy_of(i):
+    pl.semaphore_wait(barrier, n // 2)
+
+    def along(i):
         return pltpu.make_async_remote_copy(
             src_ref=own_ref,
             dst_ref=out_ref.at[me],
             send_sem=send_sem.at[i],
             recv_sem=recv_sem.at[i],
-            device_id=(lax.rem(me + i, n), tp),
+            device_id=(lax.rem(me + 2 * i, n), tp),
             device_id_type=MESH,
         )
 
+    def across(i, src):
+        return pltpu.make_async_remote_copy(
+            src_ref=src,
+            dst_ref=out_ref.at[lax.rem(me + n - 2 * i, n)],
+            send_sem=pass_sem.at[i],
+            recv_sem=take_sem.at[i],
+            device_id=(pair, tp),
+            device_id_type=MESH,
+        )
+
+    def relay(i):
+        return across(i, out_ref.at[lax.rem(me + n - 2 * i, n)])
+
     def start(i, carry):
-        copy_of(i).start()
+        along(i).start()
         return carry
 
+    def forward(i, carry):
+        along(i).wait_recv()
+        relay(i).start()
+        return carry
+
     def finish(i, carry):
-        copy_of(i).wait()
+        along(i).wait_send()
+        relay(i).wait()
         return carry
 
-    lax.fori_loop(1, n, start, 0)
+    lax.fori_loop(1, n // 2, start, 0)
+    across(0, own_ref).start()
     keep.wait()
-    lax.fori_loop(1, n, finish, 0)
+    lax.fori_loop(1, n // 2, forward, 0)
+    across(0, own_ref).wait()
+    lax.fori_loop(1, n // 2, finish, 0)
 
 
 def gather_sp(block):
@@ -139,8 +163,10 @@
         in_specs=[pl.BlockSpec(memory_space=pltpu.VMEM)],
         out_specs=pl.BlockSpec(memory_space=pltpu.VMEM),
         scratch_shapes=[
-            pltpu.SemaphoreType.DMA((n,)),
-            pltpu.SemaphoreType.DMA((n,)),
+            pltpu.SemaphoreType.DMA((n // 2,)),
+            pltpu.SemaphoreType.DMA((n // 2,)),
+            pltpu.SemaphoreType.DMA((n // 2,)),
+            pltpu.SemaphoreType.DMA((n // 2,)),
             pltpu.SemaphoreType.DMA,
         ],
         compiler_params=pltpu.CompilerParams(collective_id=0, has_side_effects=True),

time: 144 us -> 138 us (0.958)
  Pallas kernels: 130 us -> 124 us
    pallas_call x1, Pallas kernels: 106 us -> 99.8 us  [experts_layer(): pl.pallas_call(experts_kernel, out_shape=jax.ShapeDtypeStruct((tok, width...]
where the time goes in v2:
time: 138 us; the launch traced here: 137 us
  Pallas kernels  124 us (90%)
  local copies, waits for them, and re-layouts  6.26 us (5%)
  other arithmetic  3.31 us (2%)
  matrix products  3.2 us (2%)
    pallas_call x1, Pallas kernels, experts_layer(): pl.pallas_call(experts_kernel, out_shape=jax.ShapeDtypeStruct((tok, width...  99.8 us
    pallas_call x1, Pallas kernels, gather_sp(): pl.pallas_call(functools.partial(gather_kernel, n), out_shape=jax.ShapeDt...  24.5 us
    unnamed x15, local copies, waits for them, and re-layouts  4.52 us

profile of v2, /device:TPU:0, one launch (start us, length us, event | category | flops | bytes accessed | tf_op | source)
XLA Modules:
  0.0 137.3 jit_solution(2355510117371056078)
XLA Ops:
  0.0 0.0 copy-start.1
  0.0 0.0 copy-start.4
  0.0 0.9 copy.62
  0.9 1.0 copy.42
  1.9 0.7 fusion.22
  2.7 0.1 broadcast_multiply_fusion.1
  2.8 0.1 fusion.24
  3.0 0.1 copy.43
  3.1 0.7 pad_maximum_fusion.own_ref
  3.7 24.5 %gather_kv.1 = bf16[8,128,512]{2,1,0:T(8,128)(2,1)} custom-call(bf16[128,512]{1,0:T(8,128)(2,1)} %pad_maximum_fusion.own_ref), custom_call_target="tpu_custom_call" | custom-call | bytes 16777216 | tf_op jit(solution)/shard_map/gather_kv/pallas_call | solution.py:160
  28.2 1.3 fusion.27
  29.5 0.2 copy.48
  29.7 0.2 copy.59
  29.9 0.0 copy-done.1
  29.9 0.2 copy.45
  30.2 0.1 fusion.18
  30.2 0.0 copy-done.4
  30.3 0.1 fusion.19
  30.4 0.1 multiply_subtract_fusion
  30.5 0.1 fusion.20
  30.5 0.8 bitcast_reduce_fusion
  31.3 0.0 copy-start
  31.3 0.6 fusion.1
  31.9 0.0 copy-start.2
  31.9 0.0 copy-start.3
  31.9 0.9 fusion.15
  32.9 0.6 copy-done
  33.5 1.5 %convolution_convert_fusion = bf16[128,2048]{1,0:T(8,128)(2,1)} fusion(bf16[128,1024]{0,1:T(8,128)(2,1)S(1)} %bitcast.74, bf16[1024,2048]{1,0:T(8,128)(2,1)S(1)} %copy-done), kind=kOutput, calls=%fused_computation.5 | convolution fusion | flops 537133056 | bytes 4980736 | tf_op jit(solution)/shard_map/dot_general | solution.py:515
  35.0 0.0 copy-done.2
  35.0 0.0 copy-done.3
  35.1 0.1 copy.50
  35.1 0.1 copy.51
  35.2 0.7 pad_maximum_fusion.3.tail
  35.9 99.8 %experts_layer.1 = bf16[32,2048]{1,0:T(8,128)(2,1)} custom-call(bf16[4,32,2048]{2,1,0:T(8,128)(2,1)} %bitcast.68, bf16[32,2048]{1,0:T(8,128)(2,1)} %residual.1, f32[1,2048]{1,0:T(1,128)} %bitcast.78, f32[1,2048]{1,0:T(1,128)} %bitcast.79, f32[1,2048]{1,0:T(1,128)} %bitcast.80, bf16[32,128]{1,0:T(8,128)(2,1)} %pad_maximum_fusion.3.tail, ...), custom_call_target="tpu_custom_call" | custom-call | tf_op jit(solution)/shard_map/experts_layer/pallas_call | solution.py:403
  135.7 1.6 %copy.64 = bf16[32,2048]{1,0:T(8,128)(2,1)} copy(bf16[32,2048]{1,0:T(8,128)(2,1)} %experts_layer.1) | data formatting | bytes 262144
  (13 shorter events, 0.1 us)
Async XLA Ops:
  0.0 29.9 %copy-start.1 = (bf16[128,8,128]{2,1,0:T(8,128)(2,1)S(1)}, bf16[128,8,128]{2,1,0:T(8,128)(2,1)}, u32[]{:S(2)}) copy-start(bf16[128,8,128]{2,1,0:T(8,128)(2,1)} %param.15) | copy-start | bytes 786436
  0.0 30.2 %copy-start.4 = (f32[128]{0:T(128)S(1)}, f32[128]{0:T(128)}, u32[]{:S(2)}) copy-start(f32[128]{0:T(128)} %param.18) | copy-start | bytes 1540
  31.3 2.2 %copy-start = (bf16[1024,2048]{1,0:T(8,128)(2,1)S(1)}, bf16[1024,2048]{1,0:T(8,128)(2,1)}, u32[]{:S(2)}) copy-start(bf16[1024,2048]{1,0:T(8,128)(2,1)} %param.20) | copy-start | bytes 12582916
  31.9 3.1 %copy-start.2 = (f32[32,4]{0,1:T(4,128)S(1)}, f32[32,4]{0,1:T(4,128)}, u32[]{:S(2)}) copy-start(f32[32,4]{0,1:T(4,128)} %param.25) | copy-start | bytes 1540
  31.9 3.1 %copy-start.3 = (s32[32,4]{0,1:T(4,128)S(1)}, s32[32,4]{0,1:T(4,128)}, u32[]{:S(2)}) copy-start(s32[32,4]{0,1:T(4,128)} %param.24) | copy-start | bytes 1540
